TPU v7x, 32 devices: a whole 2x2x4 slice. The times are simulated.
32 devices in a mesh: ep: 8 (over z, x), tp: 4 (over y, core).
Axes of the slice: x: 2, y: 2, z: 4, core: 2. Of those that a mesh axis runs over, the one named last changes fastest.
Arguments:
- tokens: bfloat16 [192, 4096], P('ep'), may hold values from -6 to 6
- norm_gain: bfloat16 [4096], replicated, may hold values from 0.099609375 to 1.8984375
- w_query: bfloat16 [4096, 1024], P('ep', 'tp'), may hold values from -0.09375 to 0.09375
- w_key: bfloat16 [4096, 1024], P('ep', 'tp'), may hold values from -0.09375 to 0.09375
- w_value: bfloat16 [4096, 2048], P('ep', 'tp'), may hold values from -0.09375 to 0.09375
- w_rgate: bfloat16 [4096, 2048], P('ep', 'tp'), may hold values from -0.09375 to 0.09375
- w_decay: bfloat16 [4096, 1024], P('ep', 'tp'), may hold values from -0.375 to 0.375
- decay_shift: float32 [192, 1024], P('ep', 'tp'), may hold values from -2 to 0
- state: float32 [192, 8, 128, 256], P('ep', 'tp'), may hold values from -6 to 6
- head_gain: bfloat16 [2048], P('tp'), may hold values from 0.099609375 to 1.8984375
- w_out: bfloat16 [2048, 4096], P('tp', 'ep'), may hold values from -0.125 to 0.125
- ffn_gain: bfloat16 [4096], replicated, may hold values from 0.099609375 to 1.8984375
- w_gate: bfloat16 [8, 4096, 1024], P('ep', None, 'tp'), may hold values from -0.21875 to 0.21875
- w_lin: bfloat16 [8, 4096, 1024], P('ep', None, 'tp'), may hold values from -0.21875 to 0.21875
- w_down: bfloat16 [8, 1024, 4096], P('ep', 'tp'), may hold values from -0.046875 to 0.046875
- expert_ids: int32 [192, 4], P('ep'), may hold values from 0 to 7, all different within a row; in each aligned block of 24 rows (0 to 23, 24 to 47, ...) at most 24 rows name the same one
- route_weight: float32 [192, 4], P('ep'), may hold values from 0.2 to 1
Outputs:
- result: bfloat16 [192, 4096], P('ep')
Inputs may be any that keep to these rules, and one draw needn't show every extreme that they name: `expert_ids`: each row names 4 different experts; among the rows of one index of ep no expert is named more than 24 times, a bound that some block reaches.
All inputs are finite; a program needn't handle non-finite values.
Results may differ from a plain program's by a relative error of at most 0.022.
Values may be sent and summed in bfloat16 or wider, within the bound.
A program may use at most 128 MiB of HBM per device.

v0:
```python
import jax
import jax.numpy as jnp
from jax import lax
from jax.sharding import PartitionSpec as P

eps = 1e-06
tau = 16.0
limit = 7.0
glu_alpha = 1.702


def rms_scale(values, gain):
    meansq = jnp.mean(values * values, axis=-1, keepdims=True)
    return values * lax.rsqrt(meansq + eps) * gain


def activate(gate, linear):
    gate = jnp.minimum(gate, limit)
    linear = jnp.clip(linear, -limit, limit)
    return (gate * jax.nn.sigmoid(glu_alpha * gate) * (linear + 1.0)).astype(jnp.bfloat16)


def on_device(
    tokens,
    norm_gain,
    w_query,
    w_key,
    w_value,
    w_rgate,
    w_decay,
    decay_shift,
    state,
    head_gain,
    w_out,
    ffn_gain,
    w_gate,
    w_lin,
    w_down,
    expert_ids,
    route_weight,
):
    seq_dev = tokens.shape[0]
    width = tokens.shape[1]
    heads_dev = state.shape[1]
    key_dim = state.shape[2]
    val_dim = state.shape[3]
    key_cols = w_query.shape[1]
    val_cols = w_value.shape[1]
    inputs = tokens.astype(jnp.float32)
    normed = rms_scale(inputs, norm_gain.astype(jnp.float32)).astype(jnp.bfloat16)
    spread = lax.all_to_all(normed, "ep", split_axis=1, concat_axis=0, tiled=True)
    joined = jnp.concatenate((w_query, w_key, w_decay, w_value, w_rgate), axis=1)
    projected = lax.psum_scatter(
        jnp.dot(spread, joined, preferred_element_type=jnp.float32),
        "ep",
        scatter_dimension=0,
        tiled=True,
    )
    projected = projected.astype(jnp.bfloat16).astype(jnp.float32)
    q_rows = projected[:, :key_cols].reshape(seq_dev, heads_dev, key_dim) * key_dim ** (-0.5)
    k_rows = projected[:, key_cols : 2 * key_cols].reshape(seq_dev, heads_dev, key_dim)
    decay_pre = projected[:, 2 * key_cols : 3 * key_cols]
    v_rows = projected[:, 3 * key_cols : 3 * key_cols + val_cols].reshape(
        seq_dev, heads_dev, val_dim
    )
    rgates = projected[:, 3 * key_cols + val_cols :].reshape(seq_dev, heads_dev, val_dim)
    log_decay = jax.nn.log_sigmoid(decay_pre) / tau + decay_shift
    new_state = (
        jnp.exp(log_decay.reshape(seq_dev, heads_dev, key_dim))[..., None] * state
        + k_rows[..., None] * v_rows[:, :, None, :]
    )
    read = jnp.einsum("shk,shkv->shv", q_rows, new_state, precision=lax.Precision.HIGHEST)
    gated = rms_scale(
        read, head_gain.astype(jnp.float32).reshape(heads_dev, val_dim)
    ) * jax.nn.silu(rgates)
    gated = gated.reshape(seq_dev, heads_dev * val_dim).astype(jnp.bfloat16)
    partial_value = jnp.dot(
        lax.all_gather(gated, "ep", axis=0, tiled=True), w_out, preferred_element_type=jnp.float32
    )
    summed = lax.psum(partial_value.astype(jnp.bfloat16), "tp")
    mixed = lax.all_to_all(summed, "ep", split_axis=0, concat_axis=1, tiled=True)
    stream = inputs + mixed.astype(jnp.float32)
    ffn_in = rms_scale(stream, ffn_gain.astype(jnp.float32)).astype(jnp.bfloat16)
    n_ep = lax.axis_size("ep")
    exp_dev = w_gate.shape[0]
    experts = exp_dev * n_ep
    top = expert_ids.shape[1]
    capacity = max(2, 2 * seq_dev * top // experts)
    flat_ids = expert_ids.reshape(-1)
    onehot = (flat_ids[:, None] == jnp.arange(experts, dtype=jnp.int32)[None, :]).astype(jnp.int32)
    rank = jnp.sum((jnp.cumsum(onehot, axis=0) - onehot) * onehot, axis=1)
    slot_of = flat_ids * capacity + rank
    dispatch = (
        jnp.arange(experts * capacity, dtype=jnp.int32)[:, None] == slot_of[None, :]
    ).astype(jnp.bfloat16)
    dispatch = jnp.sum(dispatch.reshape(experts * capacity, seq_dev, top), axis=2)
    outbound = jnp.dot(dispatch, ffn_in, preferred_element_type=jnp.float32).astype(jnp.bfloat16)
    outbound = outbound.reshape(experts, capacity, width)
    arrived = lax.all_to_all(outbound, "ep", split_axis=0, concat_axis=0, tiled=True)
    count = arrived.shape[1]
    rows = arrived.reshape(n_ep, exp_dev, count, width)
    gate = jnp.einsum("secd,edh->sech", rows, w_gate, preferred_element_type=jnp.float32)
    linear = jnp.einsum("secd,edh->sech", rows, w_lin, preferred_element_type=jnp.float32)
    act = activate(gate, linear)
    partial_out = jnp.einsum("sech,ehd->secd", act, w_down, preferred_element_type=jnp.float32)
    summed_out = lax.psum(partial_out.astype(jnp.bfloat16), "tp")
    returned = lax.all_to_all(
        summed_out.reshape(n_ep * exp_dev, count, width),
        "ep",
        split_axis=0,
        concat_axis=0,
        tiled=True,
    )
    picked = (
        returned.reshape(experts * capacity, width)[slot_of]
        .astype(jnp.float32)
        .reshape(seq_dev, top, width)
    )
    routed = jnp.sum(picked * route_weight[..., None], axis=1)
    return (stream + routed).astype(jnp.bfloat16)


def solution(mesh):
    placed = (
        P("ep", None),
        P(),
        P("ep", "tp"),
        P("ep", "tp"),
        P("ep", "tp"),
        P("ep", "tp"),
        P("ep", "tp"),
        P("ep", "tp"),
        P("ep", "tp", None, None),
        P("tp"),
        P("tp", "ep"),
        P(),
        P("ep", None, "tp"),
        P("ep", None, "tp"),
        P("ep", "tp", None),
        P("ep", None),
        P("ep", None),
    )
    return jax.shard_map(
        on_device, mesh=mesh, in_specs=placed, out_specs=P("ep", None), check_vma=False
    )
```

profile of v0, /device:TPU:0, one launch (start us, length us, event | category | flops | bytes accessed | tf_op | source)
XLA Modules:
  0.0 322.8 jit_solution(11763685602241706706)
XLA Ops:
  7.4 1.1 fusion.38
  8.5 1.1 fusion.40
  10.3 7.3 %all-to-all-start = ((bf16[24,8,512]{2,0,1:T(8,128)(2,1)}), bf16[24,8,512]{2,0,1:T(8,128)(2,1)S(1)}, u32[]{:S(2)}, u32[]{:S(2)}) async-start(bf16[24,8,512]{2,0,1:T(8,128)(2,1)} %bitcast.95), calls=%async_computation | async-start | bytes 393216 | tf_op jit(solution)/shard_map/all_to_all | solution.py:51
  17.6 1.7 constant_dynamic-update-slice_fusion.4
  19.3 1.7 constant_dynamic-update-slice_fusion.3
  21.0 1.7 constant_dynamic-update-slice_fusion.2
  24.5 1.0 all-to-all-done
  25.5 3.2 fusion.72
  29.0 65.7 %reduce-scatter.2.cloned.1.call-done = f32[24,1792]{1,0:T(8,128)} async-done(((f32[192,1792]{1,0:T(8,128)}), f32[24,1792]{1,0:T(8,128)}) %reduce-scatter.2.cloned.1.call-update) | async-done | bytes 172048 | tf_op jit(solution)/shard_map/reduce_scatter | solution.py:53
  95.8 6.1 %fusion = f32[24,2,1,256]{3,2,1,0:T(1,128)S(1)} fusion(f32[24,2,128,1]{2,3,1,0:T(1,128)S(1)} %bitcast.103, f32[24,2,128,256]{3,2,1,0:T(8,128)} %param.25, f32[24,2,256]{2,1,0:T(2,128)S(1)} %mul.158, f32[24,2,128]{2,1,0:T(2,128)S(1)} %mul.156, f32[24,2,128]{2,1,0:T(2,128)S(1)} %exp.24), kind=kOutput, calls=%fused_computation.1 | convolution fusion | flops 23592960 | bytes 6463488 | tf_op jit(solution)/shard_map/shk,shkv->shv/dot_general | solution.py:72
  102.2 30.6 %all_gather.3 = bf16[192,512]{1,0:T(8,128)(2,1)S(1)} all-gather(bf16[24,512]{1,0:T(8,128)(2,1)S(1)} %bitcast.104), channel_id=1, replica_groups=mesh['ep'=8,'tp'=4] {'ep'}, dimensions={0}, use_global_device_ids=true | all-gather | bytes 221184 | tf_op jit(solution)/shard_map/all_gather | solution.py:78
  132.9 1.0 convolution_convert_fusion.2
  134.1 30.6 %all-reduce.3.cloned.1.call-done = bf16[8,24,512]{2,1,0:T(8,128)(2,1)} async-done(((bf16[8,24,512]{2,1,0:T(8,128)(2,1)}), bf16[8,24,512]{2,1,0:T(8,128)(2,1)}) %all-reduce.3.cloned.1.call-update) | async-done | bytes 196624 | tf_op jit(solution)/shard_map/psum | solution.py:80
  164.6 5.5 %all-to-all-start.1 = ((bf16[8,24,512]{2,1,0:T(8,128)(2,1)}), bf16[8,24,512]{2,1,0:T(8,128)(2,1)S(1)}, u32[]{:S(2)}, u32[]{:S(2)}) async-start(bf16[8,24,512]{2,1,0:T(8,128)(2,1)} %all-reduce.3.cloned.1.call-done), calls=%async_computation.2 | async-start | bytes 393216 | tf_op jit(solution)/shard_map/all_to_all | solution.py:81
  170.7 7.3 %all-to-all-done.1 = bf16[8,24,512]{2,1,0:T(8,128)(2,1)S(1)} async-done(((bf16[8,24,512]{2,1,0:T(8,128)(2,1)}), bf16[8,24,512]{2,1,0:T(8,128)(2,1)S(1)}, u32[]{:S(2)}, u32[]{:S(2)}) %all-to-all-start.1) | async-done | bytes 196640 | tf_op jit(solution)/shard_map/all_to_all | solution.py:81
  178.9 37.3 %all_to_all.42 = bf16[8,24,4096]{2,1,0:T(8,128)(2,1)S(1)} all-to-all(bf16[8,24,4096]{2,1,0:T(8,128)(2,1)S(1)} %bitcast.96), channel_id=1, replica_groups=mesh['ep'=8,'tp'=4] {'ep'}, dimensions={0} | all-to-all | bytes 3145728 | tf_op jit(solution)/shard_map/all_to_all | solution.py:99
  216.2 1.2 copy-done.1
  218.0 5.1 %convolution_convert_fusion = bf16[8,24,4096]{2,1,0:T(8,128)(2,1)} fusion(bf16[1,256,4096]{2,1,0:T(8,128)(2,1)S(1)} %copy-done, bf16[8,24,4096]{2,1,0:T(8,128)(2,1)} %copy-done.1, bf16[1,4096,256]{2,1,0:T(8,128)(2,1)} %param.30, f32[8,1,24,256]{3,2,0,1:T(8,128)S(1)} %fusion.27), kind=kOutput, calls=%fused_computation.5 | convolution fusion | flops 806535168 | bytes 7536640 | tf_op jit(solution)/shard_map/sech,ehd->secd/dot_general | solution.py:105
  223.1 42.3 %all-reduce.5.cloned.1.call-done = bf16[8,24,4096]{2,1,0:T(8,128)(2,1)} async-done(((bf16[8,24,4096]{2,1,0:T(8,128)(2,1)}), bf16[8,24,4096]{2,1,0:T(8,128)(2,1)}) %all-reduce.5.cloned.1.call-update) | async-done | bytes 1572880 | tf_op jit(solution)/shard_map/psum | solution.py:106
  265.5 5.5 %all-to-all-start.3 = ((bf16[8,24,4096]{2,1,0:T(8,128)(2,1)}), bf16[8,24,4096]{2,1,0:T(8,128)(2,1)}, u32[]{:S(2)}, u32[]{:S(2)}) async-start(bf16[8,24,4096]{2,1,0:T(8,128)(2,1)} %all-reduce.5.cloned.1.call-done), calls=%async_computation.4 | async-start | bytes 3145728 | tf_op jit(solution)/shard_map/all_to_all | solution.py:107
  271.2 36.8 %all-to-all-done.3 = bf16[8,24,4096]{2,1,0:T(8,128)(2,1)} async-done(((bf16[8,24,4096]{2,1,0:T(8,128)(2,1)}), bf16[8,24,4096]{2,1,0:T(8,128)(2,1)}, u32[]{:S(2)}, u32[]{:S(2)}) %all-to-all-start.3) | async-done | bytes 1572896 | tf_op jit(solution)/shard_map/all_to_all | solution.py:107
  308.0 3.4 %gather_fusion = bf16[96,4096]{1,0:T(8,128)(2,1)S(1)} fusion(bf16[192,4096]{1,0:T(8,128)(2,1)} %bitcast.22, s32[1024]{0:T(1024)S(1)} %pad_clamp_fusion), kind=kCustom, calls=%fused_computation | custom fusion | bytes 1573248 | tf_op jit(solution)/shard_map/gather | solution.py:115
  311.4 1.6 reshape.151
  313.0 2.5 multiply_reduce_fusion
  (68 shorter events, 8.2 us)
Async XLA Ops:
  6.5 211.5 %copy-start = (bf16[1,256,4096]{2,1,0:T(8,128)(2,1)S(1)}, bf16[1,256,4096]{2,1,0:T(8,128)(2,1)}, u32[]{:S(2)}) copy-start(bf16[1,256,4096]{2,1,0:T(8,128)(2,1)} %param.31) | copy-start | bytes 6291460
  6.5 16.1 %copy-start.5 = (bf16[512,512]{1,0:T(8,128)(2,1)S(1)}, bf16[512,512]{1,0:T(8,128)(2,1)}, u32[]{:S(2)}) copy-start(bf16[512,512]{1,0:T(8,128)(2,1)} %param.21) | copy-start | bytes 1572868
  8.5 15.1 %copy-start.6 = (bf16[512,512]{1,0:T(8,128)(2,1)S(1)}, bf16[512,512]{1,0:T(8,128)(2,1)}, u32[]{:S(2)}) copy-start(bf16[512,512]{1,0:T(8,128)(2,1)} %param.22) | copy-start | bytes 1572868
  10.3 15.2 %all-to-all-start = ((bf16[24,8,512]{2,0,1:T(8,128)(2,1)}), bf16[24,8,512]{2,0,1:T(8,128)(2,1)S(1)}, u32[]{:S(2)}, u32[]{:S(2)}) async-start(bf16[24,8,512]{2,0,1:T(8,128)(2,1)} %bitcast.95), calls=%async_computation | async-start | bytes 393216 | tf_op jit(solution)/shard_map/all_to_all | solution.py:51
  17.6 77.2 %reduce-scatter.2.cloned.1.call-start = ((), (), s32[]{:S(2)}) async-start(), calls=%async_computation.5 | async-start | bytes 1548288 | tf_op jit(solution)/shard_map/reduce_scatter | solution.py:53
  25.5 3.2 %copy-start.11 = (bf16[512]{0:T(512)(128)(2,1)S(1)}, bf16[512]{0:T(512)(128)(2,1)}, u32[]{:S(2)}) copy-start(bf16[512]{0:T(512)(128)(2,1)} %param.26) | copy-start | bytes 3076
  25.5 3.3 %copy-start.9 = (s32[24,4]{0,1:T(4,128)S(1)}, s32[24,4]{0,1:T(4,128)}, u32[]{:S(2)}) copy-start(s32[24,4]{0,1:T(4,128)} %param.32) | copy-start | bytes 1156
  25.5 70.2 %copy-start.7 = (f32[24,256]{1,0:T(8,128)S(1)}, f32[24,256]{1,0:T(8,128)}, u32[]{:S(2)}) copy-start(f32[24,256]{1,0:T(8,128)} %param.24) | copy-start | bytes 73732
  28.7 135.9 %all-reduce.3.cloned.1.call-start = ((), (), s32[]{:S(2)}) async-start(), calls=%async_computation.6 | async-start | bytes 393216 | tf_op jit(solution)/shard_map/psum | solution.py:80
  95.8 37.0 %copy-start.4 = (bf16[512,512]{1,0:T(8,128)(2,1)S(1)}, bf16[512,512]{1,0:T(8,128)(2,1)}, u32[]{:S(2)}) copy-start(bf16[512,512]{1,0:T(8,128)(2,1)} %param.27) | copy-start | bytes 1572868
  101.9 68.7 %copy-start.8 = (bf16[4096]{0:T(1024)(128)(2,1)S(1)}, bf16[4096]{0:T(1024)(128)(2,1)}, u32[]{:S(2)}) copy-start(bf16[4096]{0:T(1024)(128)(2,1)} %param.28) | copy-start | bytes 24580
  102.1 76.0 %copy-start.2 = (bf16[24,4096]{1,0:T(8,128)(2,1)S(1)}, bf16[24,4096]{1,0:T(8,128)(2,1)}, u32[]{:S(2)}) copy-start(bf16[24,4096]{1,0:T(8,128)(2,1)} %param.17) | copy-start | bytes 589828
  164.6 13.3 %all-to-all-start.1 = ((bf16[8,24,512]{2,1,0:T(8,128)(2,1)}), bf16[8,24,512]{2,1,0:T(8,128)(2,1)S(1)}, u32[]{:S(2)}, u32[]{:S(2)}) async-start(bf16[8,24,512]{2,1,0:T(8,128)(2,1)} %all-reduce.3.cloned.1.call-done), calls=%async_computation.2 | async-start | bytes 393216 | tf_op jit(solution)/shard_map/all_to_all | solution.py:81
  170.2 95.3 %all-reduce.5.cloned.1.call-start = ((), (), s32[]{:S(2)}) async-start(), calls=%async_computation.7 | async-start | bytes 3145728 | tf_op jit(solution)/shard_map/psum | solution.py:106
  178.8 38.5 %copy-start.3 = (bf16[1,4096,256]{2,1,0:T(8,128)(2,1)S(1)}, bf16[1,4096,256]{2,1,0:T(8,128)(2,1)}, u32[]{:S(2)}) copy-start(bf16[1,4096,256]{2,1,0:T(8,128)(2,1)} %param.29) | copy-start | bytes 6291460
  216.2 1.2 copy-start.1
  223.1 47.9 %copy-start.10 = (f32[24,4]{0,1:T(4,128)S(1)}, f32[24,4]{0,1:T(4,128)}, u32[]{:S(2)}) copy-start(f32[24,4]{0,1:T(4,128)} %param.33) | copy-start | bytes 1156
  265.5 42.5 %all-to-all-start.3 = ((bf16[8,24,4096]{2,1,0:T(8,128)(2,1)}), bf16[8,24,4096]{2,1,0:T(8,128)(2,1)}, u32[]{:S(2)}, u32[]{:S(2)}) async-start(bf16[8,24,4096]{2,1,0:T(8,128)(2,1)} %all-reduce.5.cloned.1.call-done), calls=%async_computation.4 | async-start | bytes 3145728 | tf_op jit(solution)/shard_map/all_to_all | solution.py:107
Sparse Core Ops, SparseCore 0:
  28.8 65.8 reduce-scatter.1
  134.0 30.6 all-reduce.2
  223.2 42.1 all-reduce.4
where the time goes:
time: 323 us
  waiting for transfers between devices  184 us (57%)
  blocking collectives  68 us (21%)
  starting transfers between devices  18.4 us (6%)
  matrix products  16.5 us (5%)
  local copies, waits for them, and re-layouts  14.5 us (4%)
  between operations  13.4 us (4%)
  other arithmetic  8.18 us (3%)
    reduce_scatter x1, waiting for transfers between devices, on_device(): lax.psum_scatter(jnp.dot(spread, joined, preferred_element_type=jnp.float...  65.7 us
    psum x1, waiting for transfers between devices, on_device(): summed_out = lax.psum(partial_out.astype(jnp.bfloat16), 'tp')  42.3 us
    all_to_all x1, blocking collectives, on_device(): lax.all_to_all(outbound, 'ep', split_axis=0, concat_axis=0, tiled=True)  37.3 us
    all_to_all x1, waiting for transfers between devices, on_device(): lax.all_to_all(summed_out.reshape(n_ep * exp_dev, count, width), 'ep', sp...  36.8 us
    all_gather x1, blocking collectives, on_device(): lax.all_gather(gated, 'ep', axis=0, tiled=True)  30.6 us
    psum x1, waiting for transfers between devices, on_device(): summed = lax.psum(partial_value.astype(jnp.bfloat16), 'tp')  30.6 us
    unnamed x31, local copies, waits for them, and re-layouts  7.35 us
    all_to_all x1, starting transfers between devices, on_device(): lax.all_to_all(normed, 'ep', split_axis=1, concat_axis=0, tiled=True)  7.28 us
  transfers between devices with their start and end apart: 6, of which 6 were waited for; matrix products, arithmetic and copies ran while one was open for 2% of the time, Pallas kernels for 0%

commit v1 on v0

--- a/solution.py
+++ b/solution.py
@@ -77,7 +77,9 @@
     partial_value = jnp.dot(
         lax.all_gather(gated, "ep", axis=0, tiled=True), w_out, preferred_element_type=jnp.float32
     )
-    summed = lax.psum(partial_value.astype(jnp.bfloat16), "tp")
+    own = partial_value.astype(jnp.bfloat16)
+    parts = lax.all_gather(own, "tp")
+    summed = jnp.sum(parts, axis=0)
     mixed = lax.all_to_all(summed, "ep", split_axis=0, concat_axis=1, tiled=True)
     stream = inputs + mixed.astype(jnp.float32)
     ffn_in = rms_scale(stream, ffn_gain.astype(jnp.float32)).astype(jnp.bfloat16)

time: 323 us -> 302 us (0.935)
  waiting for transfers between devices: 184 us -> 153 us
  blocking collectives: 68 us -> 79.5 us
    psum x1 -> x0, waiting for transfers between devices: 30.6 us -> none  [on_device(): summed = lax.psum(partial_value.astype(jnp.bfloat16), 'tp')]
    all_gather x0 -> x1, blocking collectives: none -> 8.7 us  [on_device(): parts = lax.all_gather(own, 'tp')]
  transfers between devices with their start and end apart: 6 -> 5, of which waited for: 6 -> 5; matrix products, arithmetic and copies ran while one was open for 2% -> 3% of each run, Pallas kernels for 0% -> 0%
where the time goes in v1:
time: 302 us
  waiting for transfers between devices  153 us (51%)
  blocking collectives  79.5 us (26%)
  starting transfers between devices  16.3 us (5%)
  matrix products  15.8 us (5%)
  local copies, waits for them, and re-layouts  14.5 us (5%)
  between operations  13.7 us (5%)
  other arithmetic  9 us (3%)
    reduce_scatter x1, waiting for transfers between devices, on_device(): lax.psum_scatter(jnp.dot(spread, joined, preferred_element_type=jnp.float...  65.5 us
    psum x1, waiting for transfers between devices, on_device(): summed_out = lax.psum(partial_out.astype(jnp.bfloat16), 'tp')  41.1 us
    all_to_all x1, blocking collectives, on_device(): lax.all_to_all(outbound, 'ep', split_axis=0, concat_axis=0, tiled=True)  40.2 us
    all_to_all x1, waiting for transfers between devices, on_device(): lax.all_to_all(summed_out.reshape(n_ep * exp_dev, count, width), 'ep', sp...  36.8 us
    all_gather x1, blocking collectives, on_device(): lax.all_gather(gated, 'ep', axis=0, tiled=True)  30.6 us
    all_gather x1, blocking collectives, on_device(): parts = lax.all_gather(own, 'tp')  8.7 us
    all_to_all x1, waiting for transfers between devices, on_device(): lax.all_to_all(summed, 'ep', split_axis=0, concat_axis=1, tiled=True)  8.16 us
    unnamed x31, local copies, waits for them, and re-layouts  7.37 us
  transfers between devices with their start and end apart: 5, of which 5 were waited for; matrix products, arithmetic and copies ran while one was open for 3% of the time, Pallas kernels for 0%

profile of v1, /device:TPU:0, one launch (start us, length us, event | category | flops | bytes accessed | tf_op | source)
XLA Modules:
  0.0 301.5 jit_solution(16738004663710420703)
XLA Ops:
  7.4 1.1 fusion.38
  8.5 1.1 fusion.40
  10.3 7.3 %all-to-all-start = ((bf16[24,8,512]{2,0,1:T(8,128)(2,1)}), bf16[24,8,512]{2,0,1:T(8,128)(2,1)S(1)}, u32[]{:S(2)}, u32[]{:S(2)}) async-start(bf16[24,8,512]{2,0,1:T(8,128)(2,1)} %bitcast.96), calls=%async_computation | async-start | bytes 393216 | tf_op jit(solution)/shard_map/all_to_all | solution.py:51
  17.6 1.7 constant_dynamic-update-slice_fusion.4
  19.3 1.7 constant_dynamic-update-slice_fusion.3
  21.0 1.7 constant_dynamic-update-slice_fusion.2
  24.4 1.1 all-to-all-done
  25.5 3.2 %fusion.72 = f32[192,1792]{1,0:T(8,128)} fusion(bf16[192,512]{1,0:T(8,128)(2,1)S(1)} %bitcast.103, bf16[512,1792]{1,0:T(8,128)(2,1)} %constant_dynamic-update-slice_fusion), kind=kOutput, calls=%fused_computation.89 | convolution fusion | flops 352321536 | bytes 3407872 | tf_op jit(solution)/shard_map/dot_general | solution.py:54
  29.2 65.5 %reduce-scatter.2.cloned.1.call-done = f32[24,1792]{1,0:T(8,128)} async-done(((f32[192,1792]{1,0:T(8,128)}), f32[24,1792]{1,0:T(8,128)}) %reduce-scatter.2.cloned.1.call-update) | async-done | bytes 172048 | tf_op jit(solution)/shard_map/reduce_scatter | solution.py:53
  94.7 0.9 convert_convert_fusion
  95.8 6.1 %fusion = f32[24,2,1,256]{3,2,1,0:T(1,128)S(1)} fusion(f32[24,2,128,1]{2,3,1,0:T(1,128)S(1)} %bitcast.104, f32[24,2,128,256]{3,2,1,0:T(8,128)} %param.25, f32[24,2,256]{2,1,0:T(2,128)S(1)} %mul.158, f32[24,2,128]{2,1,0:T(2,128)S(1)} %mul.156, f32[24,2,128]{2,1,0:T(2,128)S(1)} %exp.24), kind=kOutput, calls=%fused_computation.1 | convolution fusion | flops 23592960 | bytes 6463488 | tf_op jit(solution)/shard_map/shk,shkv->shv/dot_general | solution.py:72
  102.2 30.6 %all_gather.9 = bf16[192,512]{1,0:T(8,128)(2,1)S(1)} all-gather(bf16[24,512]{1,0:T(8,128)(2,1)S(1)} %bitcast.105), channel_id=1, replica_groups=mesh['ep'=8,'tp'=4] {'ep'}, dimensions={0}, use_global_device_ids=true | all-gather | bytes 221184 | tf_op jit(solution)/shard_map/all_gather | solution.py:78
  133.1 8.7 %all-gather = bf16[768,512]{1,0:T(8,128)(2,1)S(1)} all-gather(bf16[192,512]{1,0:T(8,128)(2,1)S(1)} %convolution_convert_fusion.2), channel_id=2, replica_groups=mesh['ep'=8,'tp'=4] {'tp'}, dimensions={0}, use_global_device_ids=true | all-gather | bytes 983040 | tf_op jit(solution)/shard_map/all_gather | solution.py:81
  142.6 3.4 %all-to-all-start.1 = ((bf16[8,24,512]{2,1,0:T(8,128)(2,1)}), bf16[8,24,512]{2,1,0:T(8,128)(2,1)S(1)}, u32[]{:S(2)}, u32[]{:S(2)}) async-start(bf16[8,24,512]{2,1,0:T(8,128)(2,1)} %bitcast.5), calls=%async_computation.2 | async-start | bytes 393216 | tf_op jit(solution)/shard_map/all_to_all | solution.py:83
  146.5 8.2 %all-to-all-done.1 = bf16[8,24,512]{2,1,0:T(8,128)(2,1)S(1)} async-done(((bf16[8,24,512]{2,1,0:T(8,128)(2,1)}), bf16[8,24,512]{2,1,0:T(8,128)(2,1)S(1)}, u32[]{:S(2)}, u32[]{:S(2)}) %all-to-all-start.1) | async-done | bytes 196640 | tf_op jit(solution)/shard_map/all_to_all | solution.py:83
  155.6 40.2 %all_to_all.42 = bf16[8,24,4096]{2,1,0:T(8,128)(2,1)S(1)} all-to-all(bf16[8,24,4096]{2,1,0:T(8,128)(2,1)S(1)} %bitcast.97), channel_id=1, replica_groups=mesh['ep'=8,'tp'=4] {'ep'}, dimensions={0} | all-to-all | bytes 3145728 | tf_op jit(solution)/shard_map/all_to_all | solution.py:101
  195.8 1.2 copy-done.1
  197.6 5.1 %convolution_convert_fusion = bf16[8,24,4096]{2,1,0:T(8,128)(2,1)} fusion(bf16[1,256,4096]{2,1,0:T(8,128)(2,1)S(1)} %copy-done, bf16[8,24,4096]{2,1,0:T(8,128)(2,1)} %copy-done.1, bf16[1,4096,256]{2,1,0:T(8,128)(2,1)} %param.30, f32[8,1,24,256]{3,2,0,1:T(8,128)S(1)} %fusion.27), kind=kOutput, calls=%fused_computation.5 | convolution fusion | flops 806535168 | bytes 7536640 | tf_op jit(solution)/shard_map/sech,ehd->secd/dot_general | solution.py:107
  202.7 41.1 %all-reduce.2.cloned.1.call-done = bf16[8,24,4096]{2,1,0:T(8,128)(2,1)} async-done(((bf16[8,24,4096]{2,1,0:T(8,128)(2,1)}), bf16[8,24,4096]{2,1,0:T(8,128)(2,1)}) %all-reduce.2.cloned.1.call-update) | async-done | bytes 1572880 | tf_op jit(solution)/shard_map/psum | solution.py:108
  243.9 5.5 %all-to-all-start.3 = ((bf16[8,24,4096]{2,1,0:T(8,128)(2,1)}), bf16[8,24,4096]{2,1,0:T(8,128)(2,1)}, u32[]{:S(2)}, u32[]{:S(2)}) async-start(bf16[8,24,4096]{2,1,0:T(8,128)(2,1)} %all-reduce.2.cloned.1.call-done), calls=%async_computation.4 | async-start | bytes 3145728 | tf_op jit(solution)/shard_map/all_to_all | solution.py:109
  249.6 36.8 %all-to-all-done.3 = bf16[8,24,4096]{2,1,0:T(8,128)(2,1)} async-done(((bf16[8,24,4096]{2,1,0:T(8,128)(2,1)}), bf16[8,24,4096]{2,1,0:T(8,128)(2,1)}, u32[]{:S(2)}, u32[]{:S(2)}) %all-to-all-start.3) | async-done | bytes 1572896 | tf_op jit(solution)/shard_map/all_to_all | solution.py:109
  286.4 3.4 %gather_fusion = bf16[96,4096]{1,0:T(8,128)(2,1)S(1)} fusion(bf16[192,4096]{1,0:T(8,128)(2,1)} %bitcast.23, s32[1024]{0:T(1024)S(1)} %pad_clamp_fusion), kind=kCustom, calls=%fused_computation | custom fusion | bytes 1573248 | tf_op jit(solution)/shard_map/gather | solution.py:117
  289.8 1.6 reshape.151
  291.4 2.5 multiply_reduce_fusion
  (67 shorter events, 8.2 us)
Async XLA Ops:
  6.5 191.0 %copy-start = (bf16[1,256,4096]{2,1,0:T(8,128)(2,1)S(1)}, bf16[1,256,4096]{2,1,0:T(8,128)(2,1)}, u32[]{:S(2)}) copy-start(bf16[1,256,4096]{2,1,0:T(8,128)(2,1)} %param.31) | copy-start | bytes 6291460
  6.5 16.2 %copy-start.5 = (bf16[512,512]{1,0:T(8,128)(2,1)S(1)}, bf16[512,512]{1,0:T(8,128)(2,1)}, u32[]{:S(2)}) copy-start(bf16[512,512]{1,0:T(8,128)(2,1)} %param.21) | copy-start | bytes 1572868
  8.5 15.1 %copy-start.6 = (bf16[512,512]{1,0:T(8,128)(2,1)S(1)}, bf16[512,512]{1,0:T(8,128)(2,1)}, u32[]{:S(2)}) copy-start(bf16[512,512]{1,0:T(8,128)(2,1)} %param.22) | copy-start | bytes 1572868
  10.3 15.2 %all-to-all-start = ((bf16[24,8,512]{2,0,1:T(8,128)(2,1)}), bf16[24,8,512]{2,0,1:T(8,128)(2,1)S(1)}, u32[]{:S(2)}, u32[]{:S(2)}) async-start(bf16[24,8,512]{2,0,1:T(8,128)(2,1)} %bitcast.96), calls=%async_computation | async-start | bytes 393216 | tf_op jit(solution)/shard_map/all_to_all | solution.py:51
  17.6 77.1 %reduce-scatter.2.cloned.1.call-start = ((), (), s32[]{:S(2)}) async-start(), calls=%async_computation.5 | async-start | bytes 1548288 | tf_op jit(solution)/shard_map/reduce_scatter | solution.py:53
  25.5 3.2 %copy-start.11 = (bf16[512]{0:T(512)(128)(2,1)S(1)}, bf16[512]{0:T(512)(128)(2,1)}, u32[]{:S(2)}) copy-start(bf16[512]{0:T(512)(128)(2,1)} %param.26) | copy-start | bytes 3076
  25.5 3.2 %copy-start.9 = (s32[24,4]{0,1:T(4,128)S(1)}, s32[24,4]{0,1:T(4,128)}, u32[]{:S(2)}) copy-start(s32[24,4]{0,1:T(4,128)} %param.32) | copy-start | bytes 1156
  28.7 67.0 %copy-start.7 = (f32[24,256]{1,0:T(8,128)S(1)}, f32[24,256]{1,0:T(8,128)}, u32[]{:S(2)}) copy-start(f32[24,256]{1,0:T(8,128)} %param.24) | copy-start | bytes 73732
  95.8 37.0 %copy-start.4 = (bf16[512,512]{1,0:T(8,128)(2,1)S(1)}, bf16[512,512]{1,0:T(8,128)(2,1)}, u32[]{:S(2)}) copy-start(bf16[512,512]{1,0:T(8,128)(2,1)} %param.27) | copy-start | bytes 1572868
  102.2 44.3 %copy-start.8 = (bf16[4096]{0:T(1024)(128)(2,1)S(1)}, bf16[4096]{0:T(1024)(128)(2,1)}, u32[]{:S(2)}) copy-start(bf16[4096]{0:T(1024)(128)(2,1)} %param.28) | copy-start | bytes 24580
  133.1 21.7 %copy-start.2 = (bf16[24,4096]{1,0:T(8,128)(2,1)S(1)}, bf16[24,4096]{1,0:T(8,128)(2,1)}, u32[]{:S(2)}) copy-start(bf16[24,4096]{1,0:T(8,128)(2,1)} %param.17) | copy-start | bytes 589828
  142.6 12.1 %all-to-all-start.1 = ((bf16[8,24,512]{2,1,0:T(8,128)(2,1)}), bf16[8,24,512]{2,1,0:T(8,128)(2,1)S(1)}, u32[]{:S(2)}, u32[]{:S(2)}) async-start(bf16[8,24,512]{2,1,0:T(8,128)(2,1)} %bitcast.5), calls=%async_computation.2 | async-start | bytes 393216 | tf_op jit(solution)/shard_map/all_to_all | solution.py:83
  146.0 97.8 %all-reduce.2.cloned.1.call-start = ((), (), s32[]{:S(2)}) async-start(), calls=%async_computation.6 | async-start | bytes 3145728 | tf_op jit(solution)/shard_map/psum | solution.py:108
  155.6 41.3 %copy-start.3 = (bf16[1,4096,256]{2,1,0:T(8,128)(2,1)S(1)}, bf16[1,4096,256]{2,1,0:T(8,128)(2,1)}, u32[]{:S(2)}) copy-start(bf16[1,4096,256]{2,1,0:T(8,128)(2,1)} %param.29) | copy-start | bytes 6291460
  195.8 1.2 copy-start.1
  202.7 46.8 %copy-start.10 = (f32[24,4]{0,1:T(4,128)S(1)}, f32[24,4]{0,1:T(4,128)}, u32[]{:S(2)}) copy-start(f32[24,4]{0,1:T(4,128)} %param.33) | copy-start | bytes 1156
  243.9 42.5 %all-to-all-start.3 = ((bf16[8,24,4096]{2,1,0:T(8,128)(2,1)}), bf16[8,24,4096]{2,1,0:T(8,128)(2,1)}, u32[]{:S(2)}, u32[]{:S(2)}) async-start(bf16[8,24,4096]{2,1,0:T(8,128)(2,1)} %all-reduce.2.cloned.1.call-done), calls=%async_computation.4 | async-start | bytes 3145728 | tf_op jit(solution)/shard_map/all_to_all | solution.py:109
Sparse Core Ops, SparseCore 0:
  28.8 65.8 reduce-scatter.1
  202.8 40.9 all-reduce.1
